TPU v7x, 32 devices: a whole 2x2x4 slice. The times are simulated.
32 devices in a mesh: ep: 8 (over z, x), tp: 4 (over y, core).
Axes of the slice: x: 2, y: 2, z: 4, core: 2. Of those that a mesh axis runs over, the one named last changes fastest.
Arguments:
- tokens: bfloat16 [128, 4096], P('ep'), may hold values from -6 to 6
- norm_gain: float32 [4096], replicated, may hold values from 0.1 to 1.9
- query_weight: bfloat16 [4096, 2048], P('ep', 'tp'), may hold values from -0.09375 to 0.09375
- key_weight: bfloat16 [4096, 256], P('ep', 'tp'), may hold values from -0.09375 to 0.09375
- value_weight: bfloat16 [4096, 256], P('ep', 'tp'), may hold values from -0.09375 to 0.09375
- forget_weight: bfloat16 [4096, 32], P('ep', 'tp'), may hold values from -0.09375 to 0.09375
- forget_bias: float32 [32], P('tp'), may hold values from -1 to 2
- kv_cache: bfloat16 [128, 1024, 4, 128], P('ep', None, 'tp'), may hold values from -256 to 256, as said below
- log_gates: float32 [128, 1024, 32], P('ep', None, 'tp'), may hold values from -258 to 0
- lengths: int32 [128], P('ep'), may hold values from 128 to 1024, as said below
- out_weight: bfloat16 [2048, 4096], P('tp', 'ep'), may hold values from -0.125 to 0.125
- mix_gain: float32 [4096], replicated, may hold values from 0.1 to 1.9
- expert_gate: bfloat16 [8, 4096, 1024], P('ep', None, 'tp'), may hold values from -0.09375 to 0.09375
- expert_up: bfloat16 [8, 4096, 1024], P('ep', None, 'tp'), may hold values from -0.09375 to 0.09375
- expert_down: bfloat16 [8, 1024, 4096], P('ep', 'tp'), may hold values from -0.1875 to 0.1875
- routes: int32 [128, 4], P('ep'), may hold values from 0 to 7, all different within a row; in each aligned block of 16 rows (0 to 15, 16 to 31, ...) at most 16 rows name the same one
- route_weights: float32 [128, 4], P('ep'), may hold values from 0.2 to 1
- dense_gate: bfloat16 [4096, 4096], P(None, 'ep'), may hold values from -0.09375 to 0.09375
- dense_up: bfloat16 [4096, 4096], P(None, 'ep'), may hold values from -0.09375 to 0.09375
- dense_down: bfloat16 [4096, 4096], P('ep', 'tp'), may hold values from -0.09375 to 0.09375
- gate_vector: float32 [4096], replicated, may hold values from -0.09375 to 0.09375
Outputs:
- layer_out: bfloat16 [128, 4096], P('ep', 'tp')
Inputs may be any that keep to these rules, and one draw needn't show every extreme that they name: `kv_cache`: keys and values of the cached positions. `lengths`: some sequence uses all 1024 cached positions in every draw. A sequence's 4 experts differ. Among the routes of the 16 sequences of one index of ep no expert appears more than 16 times, and in every draw some expert appears exactly 16 times there; every expert is chosen somewhere.
All inputs are finite; a program needn't handle non-finite values.
Results may differ from a plain program's by a relative error of at most 0.012.
The roundings to bfloat16 on the way count: a program that leaves them out, or rounds other values in their place, can miss the bound.
Values may be sent and summed in bfloat16 or wider, within the bound.
No kernel may reach another device: no remote copies, remote signals or barrier semaphores. Data moves between devices by JAX's collectives and lax.ppermute only.
A program may use at most 128 MiB of HBM per device.

v0:
```python
import jax
import jax.numpy as jnp
from jax import lax
from jax.sharding import PartitionSpec as P

EPS = 1e-06


def rms_scaled(matrix, gains):
    values = matrix.astype(jnp.float32)
    return values * lax.rsqrt(jnp.mean(values * values, axis=-1, keepdims=True) + EPS) * gains


def attend_local(queries, key_new, value_new, forget, kv_cache, log_gates, lengths):
    seqs_here, cache_len, kv_count, double_width = kv_cache.shape
    head_width = double_width // 2
    group_size = queries.shape[1] // (kv_count * head_width)
    queries = queries.reshape(seqs_here, kv_count, group_size, head_width)
    key_new = key_new.reshape(seqs_here, kv_count, head_width)
    value_new = value_new.reshape(seqs_here, kv_count, head_width)
    cached_keys = kv_cache[..., :head_width]
    cached_values = kv_cache[..., head_width:]
    score_scale = head_width ** (-0.5)
    current_position = jnp.arange(cache_len, dtype=jnp.int32)
    is_last = (current_position[None, :] == lengths[:, None] - 1)[:, :, None]
    last_gate = jnp.sum(jnp.where(is_last, log_gates, 0.0), axis=1)
    newest = last_gate + forget
    gate_bias = newest[:, None, :] - log_gates
    gate_bias = gate_bias.reshape(seqs_here, cache_len, kv_count, group_size).transpose(0, 2, 3, 1)
    past_scores = (
        jnp.einsum("skgd,slkd->skgl", queries, cached_keys, preferred_element_type=jnp.float32)
        * score_scale
        + gate_bias
    )
    is_valid = (current_position[None, :] < lengths[:, None])[:, None, None, :]
    past_scores = jnp.where(is_valid, past_scores, -jnp.inf)
    own_score = (
        jnp.einsum("skgd,skd->skg", queries, key_new, preferred_element_type=jnp.float32)
        * score_scale
    )
    highest = jnp.maximum(jnp.max(past_scores, axis=-1), own_score)
    past_exp = jnp.exp(past_scores - highest[..., None])
    own_exp = jnp.exp(own_score - highest)
    totals = jnp.sum(past_exp, axis=-1) + own_exp
    past_weights = (past_exp / totals[..., None]).astype(jnp.bfloat16)
    own_weights = (own_exp / totals).astype(jnp.bfloat16)
    mixed_values = jnp.einsum(
        "skgl,slkd->skgd", past_weights, cached_values, preferred_element_type=jnp.float32
    )
    mixed_values = (
        mixed_values
        + own_weights.astype(jnp.float32)[..., None] * value_new.astype(jnp.float32)[:, :, None, :]
    )
    return mixed_values.astype(jnp.bfloat16).reshape(seqs_here, kv_count * group_size * head_width)


def shards(
    tokens,
    norm_gain,
    query_weight,
    key_weight,
    value_weight,
    forget_weight,
    forget_bias,
    kv_cache,
    log_gates,
    lengths,
    out_weight,
    mix_gain,
    expert_gate,
    expert_up,
    expert_down,
    routes,
    route_weights,
    dense_gate,
    dense_up,
    dense_down,
    gate_vector,
):
    seq_count = tokens.shape[0]
    normed = rms_scaled(tokens, norm_gain).astype(jnp.bfloat16)
    query_cols = query_weight.shape[1]
    key_cols = key_weight.shape[1]
    columns = lax.all_to_all(normed, "ep", split_axis=1, concat_axis=0, tiled=True)
    row_block = columns
    projected = lax.psum_scatter(
        jnp.concatenate(
            [
                jnp.dot(row_block, matrix, preferred_element_type=jnp.float32)
                for matrix in (query_weight, key_weight, value_weight, forget_weight)
            ],
            axis=1,
        ),
        "ep",
        scatter_dimension=0,
        tiled=True,
    )
    queries = projected[:, :query_cols].astype(jnp.bfloat16)
    key_new = projected[:, query_cols : query_cols + key_cols].astype(jnp.bfloat16)
    value_new = projected[:, query_cols + key_cols : query_cols + 2 * key_cols].astype(jnp.bfloat16)
    forget = jax.nn.log_sigmoid(projected[:, query_cols + 2 * key_cols :] + forget_bias)
    attended = attend_local(queries, key_new, value_new, forget, kv_cache, log_gates, lengths)
    column_terms = jnp.dot(
        lax.all_gather(attended, "ep", axis=0, tiled=True),
        out_weight,
        preferred_element_type=jnp.float32,
    )
    column_total = lax.psum(column_terms, "tp")
    summed = lax.all_to_all(column_total, "ep", split_axis=0, concat_axis=1, tiled=True)
    mixed = (tokens.astype(jnp.float32) + summed).astype(jnp.bfloat16)
    second = rms_scaled(mixed, mix_gain).astype(jnp.bfloat16)
    gate_value = jax.nn.sigmoid(
        jnp.dot(second.astype(jnp.float32), gate_vector, precision=lax.Precision.HIGHEST)
    )
    experts = lax.axis_size("ep")
    top_count = routes.shape[1]
    capacity = max(2, 2 * seq_count * top_count // experts)
    flat_routes = routes.reshape(-1)
    one_hot = (flat_routes[:, None] == jnp.arange(experts, dtype=jnp.int32)[None, :]).astype(
        jnp.int32
    )
    earlier = jnp.sum((jnp.cumsum(one_hot, axis=0) - one_hot) * one_hot, axis=1)
    slot_index = (flat_routes * capacity + earlier).reshape(seq_count, top_count)
    slot_ids = jnp.arange(experts * capacity, dtype=jnp.int32)
    dispatch_map = jnp.any(slot_index[None, :, :] == slot_ids[:, None, None], axis=2).astype(
        jnp.bfloat16
    )
    outgoing = jnp.dot(dispatch_map, second, preferred_element_type=jnp.float32).astype(
        jnp.bfloat16
    )
    outgoing = outgoing.reshape(experts, capacity, second.shape[1])
    received = lax.all_to_all(outgoing, "ep", split_axis=0, concat_axis=0, tiled=True)
    sources, items, model_width = received.shape
    flat_rows = received.reshape(sources * items, model_width)
    gate_pre = jnp.dot(flat_rows, expert_gate[0], preferred_element_type=jnp.float32)
    up_pre = jnp.dot(flat_rows, expert_up[0], preferred_element_type=jnp.float32)
    hidden = (jax.nn.silu(gate_pre) * up_pre).astype(jnp.bfloat16)
    partial_rows = jnp.dot(hidden, expert_down[0], preferred_element_type=jnp.float32)
    reduced = lax.psum_scatter(partial_rows, "tp", scatter_dimension=1, tiled=True)
    replies = reduced.astype(jnp.bfloat16).reshape(sources, items, reduced.shape[1])
    returned = lax.all_to_all(replies, "ep", split_axis=0, concat_axis=0, tiled=True)
    quarter_cols = returned.shape[2]
    picked = returned.reshape(experts * capacity, quarter_cols)[slot_index.reshape(-1)]
    routed = jnp.sum(
        picked.astype(jnp.float32).reshape(seq_count, top_count, quarter_cols)
        * route_weights[:, :, None],
        axis=1,
    )
    tp_index = lax.axis_index("tp")
    piece = lax.all_gather(second, "ep", axis=0, tiled=True)
    dense_hidden = (
        jax.nn.silu(jnp.dot(piece, dense_gate, preferred_element_type=jnp.float32))
        * jnp.dot(piece, dense_up, preferred_element_type=jnp.float32)
    ).astype(jnp.bfloat16)
    row_block = dense_hidden
    dense_out = lax.psum_scatter(
        jnp.dot(row_block, dense_down, preferred_element_type=jnp.float32),
        "ep",
        scatter_dimension=0,
        tiled=True,
    )
    residual = lax.dynamic_slice_in_dim(mixed, tp_index * quarter_cols, quarter_cols, 1).astype(
        jnp.float32
    )
    return (residual + routed + gate_value[:, None] * dense_out).astype(jnp.bfloat16)


def solution(mesh):
    return jax.shard_map(
        shards,
        mesh=mesh,
        in_specs=(
            P("ep", None),
            P(),
            P("ep", "tp"),
            P("ep", "tp"),
            P("ep", "tp"),
            P("ep", "tp"),
            P("tp"),
            P("ep", None, "tp", None),
            P("ep", None, "tp"),
            P("ep"),
            P("tp", "ep"),
            P(),
            P("ep", None, "tp"),
            P("ep", None, "tp"),
            P("ep", "tp", None),
            P("ep", None),
            P("ep", None),
            P(None, "ep"),
            P(None, "ep"),
            P("ep", "tp"),
            P(),
        ),
        out_specs=P("ep", "tp"),
        check_vma=False,
    )
```

profile of v0, /device:TPU:0, one launch (start us, length us, event | category | flops | bytes accessed | tf_op | source)
XLA Modules:
  0.0 333.0 jit_solution(12179301577359732236)
XLA Ops:
  6.6 1.2 fusion.48
  7.8 1.0 fusion.50
  8.9 14.4 %all_to_all.48 = bf16[16,8,512]{2,0,1:T(8,128)(2,1)S(1)} all-to-all(bf16[16,8,512]{2,0,1:T(8,128)(2,1)S(1)} %bitcast.121), channel_id=1, replica_groups=mesh['ep'=8,'tp'=4] {'ep'}, dimensions={1} | all-to-all | bytes 262144 | tf_op jit(solution)/shard_map/all_to_all | solution.py:84
  23.3 0.8 fusion.84
  24.1 1.0 fusion.83
  25.2 1.0 fusion.82
  26.2 1.3 fusion.81
  27.5 0.9 pad_maximum_fusion
  28.4 0.7 broadcast_add_fusion
  29.1 0.2 select_reduce_fusion
  29.4 59.1 %reduce-scatter.4.cloned.1.call-done = f32[16,648]{1,0:T(8,128)} async-done(((f32[128,648]{1,0:T(8,128)}), f32[16,648]{1,0:T(8,128)}) %reduce-scatter.4.cloned.1.call-update) | async-done | bytes 41488 | tf_op jit(solution)/shard_map/reduce_scatter | solution.py:86
  88.5 0.8 convert.6
  89.4 0.1 reshape.186
  89.5 0.1 fusion.71
  89.6 0.9 fusion.69
  90.5 3.7 %fusion.80 = (f32[16,8]{1,0:T(8,128)S(1)}, f32[16,1,8,1024]{3,2,0,1:T(8,128)S(1)}) fusion(f32[16,1024,8]{1,2,0:T(8,128)S(1)} %copy-done.3, f32[16,8]{1,0:T(8,128)S(1)} %fusion.69, bf16[16,8,64]{2,1,0:T(8,128)(2,1)S(1)} %reshape.186, bf16[16,1024,1,128]{3,1,2,0:T(8,128)(2,1)} %param.28, pred[16,1024]{1,0:T(8,128)(4,1)S(1)} %iota_compare_fusion.1), kind=kOutput, calls=%fused_computation.96 | convolution fusion | flops 17432448 | bytes 5276672 | tf_op jit(solution)/shard_map/skgd,slkd->skgl/dot_general | solution.py:31
  94.2 0.2 fusion.44
  94.5 1.4 fusion.37
  95.9 0.1 reshape.191
  96.0 30.5 %all_gather.6 = bf16[128,512]{1,0:T(8,128)(2,1)S(1)} all-gather(bf16[16,512]{1,0:T(8,128)(2,1)S(1)} %reshape.191), channel_id=1, replica_groups=mesh['ep'=8,'tp'=4] {'ep'}, dimensions={0}, use_global_device_ids=true | all-gather | bytes 147456 | tf_op jit(solution)/shard_map/all_gather | solution.py:104
  126.6 0.9 fusion.85
  127.7 31.3 %all-reduce.2.cloned.1.call-done = f32[8,16,512]{2,1,0:T(8,128)} async-done(((f32[8,16,512]{2,1,0:T(8,128)}), f32[8,16,512]{2,1,0:T(8,128)}) %all-reduce.2.cloned.1.call-update) | async-done | bytes 262160 | tf_op jit(solution)/shard_map/psum | solution.py:108
  159.0 5.5 %all-to-all-start.1 = ((f32[8,16,512]{2,1,0:T(8,128)}), f32[8,16,512]{2,1,0:T(8,128)S(1)}, u32[]{:S(2)}, u32[]{:S(2)}) async-start(f32[8,16,512]{2,1,0:T(8,128)} %all-reduce.2.cloned.1.call-done), calls=%async_computation.2 | async-start | bytes 524288 | tf_op jit(solution)/shard_map/all_to_all | solution.py:109
  164.6 0.1 reduce_window_sum.11
  164.7 0.2 select_reduce_fusion.1
  165.1 0.1 fusion.67
  165.2 7.6 %all-to-all-done.1 = f32[8,16,512]{2,1,0:T(8,128)S(1)} async-done(((f32[8,16,512]{2,1,0:T(8,128)}), f32[8,16,512]{2,1,0:T(8,128)S(1)}, u32[]{:S(2)}, u32[]{:S(2)}) %all-to-all-start.1) | async-done | bytes 262176 | tf_op jit(solution)/shard_map/all_to_all | solution.py:109
  172.8 0.2 fusion.45
  173.0 0.1 fusion.47
  173.1 1.5 convolution_convert_fusion
  174.6 3.6 %all-to-all-start.2 = ((bf16[8,16,4096]{2,1,0:T(8,128)(2,1)}), bf16[8,16,4096]{2,1,0:T(8,128)(2,1)S(1)}, u32[]{:S(2)}, u32[]{:S(2)}) async-start(bf16[8,16,4096]{2,1,0:T(8,128)(2,1)} %bitcast.112), calls=%async_computation.3 | async-start | bytes 2097152 | tf_op jit(solution)/shard_map/all_to_all | solution.py:132
  178.2 0.7 all-gather.2.cloned.1.call-update
  178.9 27.4 %all-to-all-done.2 = bf16[8,16,4096]{2,1,0:T(8,128)(2,1)S(1)} async-done(((bf16[8,16,4096]{2,1,0:T(8,128)(2,1)}), bf16[8,16,4096]{2,1,0:T(8,128)(2,1)S(1)}, u32[]{:S(2)}, u32[]{:S(2)}) %all-to-all-start.2) | async-done | bytes 1048608 | tf_op jit(solution)/shard_map/all_to_all | solution.py:132
  206.3 2.0 fusion.10
  208.4 4.3 %fusion.6 = f32[128,4096]{1,0:T(8,128)} fusion(bf16[1,256,4096]{2,1,0:T(8,128)(2,1)S(1)} %copy-done, bf16[128,4096]{1,0:T(8,128)(2,1)S(1)} %bitcast.110, bf16[1,4096,256]{2,1,0:T(8,128)(2,1)} %param.34, f32[128,256]{1,0:T(8,128)S(1)} %fusion.10), kind=kOutput, calls=%fused_computation.8 | convolution fusion | flops 537067520 | bytes 7471104 | tf_op jit(solution)/shard_map/dot_general | solution.py:138
  212.7 14.0 %all-gather.2.cloned.1.call-done = bf16[128,4096]{1,0:T(8,128)(2,1)} async-done(((bf16[16,4096]{1,0:T(8,128)(2,1)}), bf16[128,4096]{1,0:T(8,128)(2,1)}) %all-gather.2.cloned.1.call-update) | async-done | bytes 1048592 | tf_op jit(solution)/shard_map/all_gather | solution.py:150
  226.7 3.3 fusion.86
  230.1 4.3 %fusion.25 = f32[128,1024]{1,0:T(8,128)} fusion(bf16[512,1024]{1,0:T(8,128)(2,1)} %param.40, bf16[128,4096]{1,0:T(8,128)(2,1)S(1)} %copy-done.2, bf16[4096,512]{1,0:T(8,128)(2,1)} %param.39, f32[128,512]{1,0:T(8,128)S(1)} %fusion.86), kind=kOutput, calls=%fused_computation.20 | convolution fusion | flops 671481856 | bytes 7077888 | tf_op jit(solution)/shard_map/dot_general | solution.py:157
  234.6 24.5 %reduce-scatter.6.cloned.1.call-done = f32[128,1024]{1,0:T(8,128)} async-done(((f32[128,4096]{1,0:T(8,128)}), f32[128,1024]{1,0:T(8,128)}) %reduce-scatter.6.cloned.1.call-update) | async-done | bytes 524304 | tf_op jit(solution)/shard_map/reduce_scatter | solution.py:139
  259.0 1.8 convert_element_type.82
  260.8 5.5 %all-to-all-start.3 = ((bf16[8,16,1024]{2,1,0:T(8,128)(2,1)}), bf16[8,16,1024]{2,1,0:T(8,128)(2,1)S(1)}, u32[]{:S(2)}, u32[]{:S(2)}) async-start(bf16[8,16,1024]{2,1,0:T(8,128)(2,1)} %bitcast.19), calls=%async_computation.5 | async-start | bytes 524288 | tf_op jit(solution)/shard_map/all_to_all | solution.py:141
  266.4 0.9 fusion.43
  267.3 8.6 %all-to-all-done.3 = bf16[8,16,1024]{2,1,0:T(8,128)(2,1)S(1)} async-done(((bf16[8,16,1024]{2,1,0:T(8,128)(2,1)}), bf16[8,16,1024]{2,1,0:T(8,128)(2,1)S(1)}, u32[]{:S(2)}, u32[]{:S(2)}) %all-to-all-start.3) | async-done | bytes 262176 | tf_op jit(solution)/shard_map/all_to_all | solution.py:141
  275.9 0.7 gather_fusion
  276.6 0.1 reshape.196
  276.7 0.2 multiply_reduce_fusion
  276.9 48.0 %reduce-scatter.8.cloned.1.call-done = f32[16,1024]{1,0:T(8,128)} async-done(((f32[128,1024]{1,0:T(8,128)}), f32[16,1024]{1,0:T(8,128)}) %reduce-scatter.8.cloned.1.call-update) | async-done | bytes 65552 | tf_op jit(solution)/shard_map/reduce_scatter | solution.py:156
  324.9 1.5 add_convert_fusion
  (57 shorter events, 1.2 us)
Async XLA Ops:
  6.5 201.8 %copy-start = (bf16[1,256,4096]{2,1,0:T(8,128)(2,1)S(1)}, bf16[1,256,4096]{2,1,0:T(8,128)(2,1)}, u32[]{:S(2)}) copy-start(bf16[1,256,4096]{2,1,0:T(8,128)(2,1)} %param.35) | copy-start | bytes 6291460
  6.5 22.8 %copy-start.12 = (s32[16]{0:T(128)S(1)}, s32[16]{0:T(128)}, u32[]{:S(2)}) copy-start(s32[16]{0:T(128)} %param.30) | copy-start | bytes 196
  6.5 22.6 %copy-start.3 = (f32[16,1024,8]{1,2,0:T(8,128)S(1)}, f32[16,1024,8]{1,2,0:T(8,128)}, u32[]{:S(2)}) copy-start(f32[16,1024,8]{1,2,0:T(8,128)} %param.29) | copy-start | bytes 1572868
  6.5 83.1 %copy-start.13 = (f32[8]{0:T(128)S(1)}, f32[8]{0:T(128)}, u32[]{:S(2)}) copy-start(f32[8]{0:T(128)} %param.27) | copy-start | bytes 100
  6.5 82.0 %reduce-scatter.4.cloned.1.call-start = ((), (), s32[]{:S(2)}) async-start(), calls=%async_computation.7 | async-start | bytes 442368 | tf_op jit(solution)/shard_map/reduce_scatter | solution.py:86
  28.3 130.7 %all-reduce.2.cloned.1.call-start = ((), (), s32[]{:S(2)}) async-start(), calls=%async_computation.8 | async-start | bytes 524288 | tf_op jit(solution)/shard_map/psum | solution.py:108
  89.5 5.0 %copy-start.1 = (bf16[16,1024,1,128]{3,1,2,0:T(8,128)(2,1)S(1)}, bf16[16,1024,1,128]{3,1,2,0:T(8,128)(2,1)}, u32[]{:S(2)}) copy-start(bf16[16,1024,1,128]{3,1,2,0:T(8,128)(2,1)} %param.28) | copy-start | bytes 12582916
  94.2 32.3 %copy-start.8 = (bf16[512,512]{1,0:T(8,128)(2,1)S(1)}, bf16[512,512]{1,0:T(8,128)(2,1)}, u32[]{:S(2)}) copy-start(bf16[512,512]{1,0:T(8,128)(2,1)} %param.31) | copy-start | bytes 1572868
  94.2 33.3 %copy-start.10 = (s32[16,4]{0,1:T(4,128)S(1)}, s32[16,4]{0,1:T(4,128)}, u32[]{:S(2)}) copy-start(s32[16,4]{0,1:T(4,128)} %param.36) | copy-start | bytes 772
  94.5 78.3 %copy-start.4 = (bf16[16,4096]{1,0:T(8,128)(2,1)S(1)}, bf16[16,4096]{1,0:T(8,128)(2,1)}, u32[]{:S(2)}) copy-start(bf16[16,4096]{1,0:T(8,128)(2,1)} %param.21) | copy-start | bytes 393220
  94.5 78.5 %copy-start.9 = (f32[4096]{0:T(1024)S(1)}, f32[4096]{0:T(1024)}, u32[]{:S(2)}) copy-start(f32[4096]{0:T(1024)} %param.32) | copy-start | bytes 49156
  159.0 13.7 %all-to-all-start.1 = ((f32[8,16,512]{2,1,0:T(8,128)}), f32[8,16,512]{2,1,0:T(8,128)S(1)}, u32[]{:S(2)}, u32[]{:S(2)}) async-start(f32[8,16,512]{2,1,0:T(8,128)} %all-reduce.2.cloned.1.call-done), calls=%async_computation.2 | async-start | bytes 524288 | tf_op jit(solution)/shard_map/all_to_all | solution.py:109
  173.0 1.6 copy-start.7
  173.1 5.1 %copy-start.5 = (bf16[16,4096]{1,0:T(8,128)(2,1)}, bf16[16,4096]{1,0:T(8,128)(2,1)S(1)}, u32[]{:S(2)}) copy-start(bf16[16,4096]{1,0:T(8,128)(2,1)S(1)} %fusion.47) | copy-start | bytes 393220
  174.6 31.8 %all-to-all-start.2 = ((bf16[8,16,4096]{2,1,0:T(8,128)(2,1)}), bf16[8,16,4096]{2,1,0:T(8,128)(2,1)S(1)}, u32[]{:S(2)}, u32[]{:S(2)}) async-start(bf16[8,16,4096]{2,1,0:T(8,128)(2,1)} %bitcast.112), calls=%async_computation.3 | async-start | bytes 2097152 | tf_op jit(solution)/shard_map/all_to_all | solution.py:132
  178.1 48.6 %all-gather.2.cloned.1.call-start = ((), (), s32[]{:S(2)}) async-start(), calls=%async_computation.10 | async-start | bytes 1179648 | tf_op jit(solution)/shard_map/all_gather | solution.py:150
  178.9 80.2 %reduce-scatter.6.cloned.1.call-start = ((), (), s32[]{:S(2)}) async-start(), calls=%async_computation.9 | async-start | bytes 2621440 | tf_op jit(solution)/shard_map/reduce_scatter | solution.py:139
  212.7 112.2 %reduce-scatter.8.cloned.1.call-start = ((), (), s32[]{:S(2)}) async-start(), calls=%async_computation.11 | async-start | bytes 589824 | tf_op jit(solution)/shard_map/reduce_scatter | solution.py:156
  226.7 3.3 copy-start.2
  230.1 4.3 %copy-start.11 = (f32[16,4]{0,1:T(4,128)S(1)}, f32[16,4]{0,1:T(4,128)}, u32[]{:S(2)}) copy-start(f32[16,4]{0,1:T(4,128)} %param.37) | copy-start | bytes 772
  230.1 36.3 %copy-start.6 = (bf16[16,4096]{1,0:T(8,128)(2,1)S(1)}, bf16[16,4096]{1,0:T(8,128)(2,1)}, u32[]{:S(2)}) copy-start(bf16[16,4096]{1,0:T(8,128)(2,1)} %copy-done.5) | copy-start | bytes 393220
  260.8 15.1 %all-to-all-start.3 = ((bf16[8,16,1024]{2,1,0:T(8,128)(2,1)}), bf16[8,16,1024]{2,1,0:T(8,128)(2,1)S(1)}, u32[]{:S(2)}, u32[]{:S(2)}) async-start(bf16[8,16,1024]{2,1,0:T(8,128)(2,1)} %bitcast.19), calls=%async_computation.5 | async-start | bytes 524288 | tf_op jit(solution)/shard_map/all_to_all | solution.py:141
Sparse Core Ops, SparseCore 0:
  28.5 60.0 reduce-scatter.3
  127.6 31.3 all-reduce.1
  181.1 45.6 all-gather.1
  229.1 29.8 reduce-scatter.5
  262.2 62.6 reduce-scatter.7
where the time goes:
time: 334 us; the launch traced here: 333 us
  waiting for transfers between devices  221 us (66%)
  blocking collectives  44.9 us (13%)
  matrix products  26.6 us (8%)
  starting transfers between devices  14.8 us (4%)
  between operations  13.5 us (4%)
  other arithmetic  10.4 us (3%)
    reduce_scatter x1, waiting for transfers between devices, shards(): lax.psum_scatter(jnp.concatenate([jnp.dot(row_block, matrix, preferred_el...  59.1 us
    reduce_scatter x1, waiting for transfers between devices, shards(): lax.psum_scatter(jnp.dot(row_block, dense_down, preferred_element_type=jn...  48 us
    psum x1, waiting for transfers between devices, shards(): column_total = lax.psum(column_terms, 'tp')  31.3 us
    all_gather x1, blocking collectives, shards(): lax.all_gather(attended, 'ep', axis=0, tiled=True)  30.5 us
    all_to_all x1, waiting for transfers between devices, shards(): lax.all_to_all(outgoing, 'ep', split_axis=0, concat_axis=0, tiled=True)  27.4 us
    reduce_scatter x1, waiting for transfers between devices, shards(): lax.psum_scatter(partial_rows, 'tp', scatter_dimension=1, tiled=True)  24.5 us
    all_to_all x1, blocking collectives, shards(): lax.all_to_all(normed, 'ep', split_axis=1, concat_axis=0, tiled=True)  14.4 us
    all_gather x1, waiting for transfers between devices, shards(): piece = lax.all_gather(second, 'ep', axis=0, tiled=True)  14 us
  transfers between devices with their start and end apart: 8, of which 8 were waited for; matrix products, arithmetic and copies ran while one was open for 6% of the time, Pallas kernels for 0%

commit v1 on v0

v1 whole, which is shorter than its diff:
```python
import jax
import jax.numpy as jnp
from jax import lax
from jax.experimental import pallas as pl
from jax.experimental.pallas import tpu as pltpu
from jax.sharding import PartitionSpec as P

EPS = 1e-06


def rms_scaled(matrix, gains):
    values = matrix.astype(jnp.float32)
    return values * lax.rsqrt(jnp.mean(values * values, axis=-1, keepdims=True) + EPS) * gains


def attend_local(queries, key_new, value_new, forget, kv_cache, log_gates, lengths):
    seqs_here, cache_len, kv_count, double_width = kv_cache.shape
    head_width = double_width // 2
    group_size = queries.shape[1] // (kv_count * head_width)
    queries = queries.reshape(seqs_here, kv_count, group_size, head_width)
    key_new = key_new.reshape(seqs_here, kv_count, head_width)
    value_new = value_new.reshape(seqs_here, kv_count, head_width)
    cached_keys = kv_cache[..., :head_width]
    cached_values = kv_cache[..., head_width:]
    score_scale = head_width ** (-0.5)
    current_position = jnp.arange(cache_len, dtype=jnp.int32)
    is_last = (current_position[None, :] == lengths[:, None] - 1)[:, :, None]
    last_gate = jnp.sum(jnp.where(is_last, log_gates, 0.0), axis=1)
    newest = last_gate + forget
    gate_bias = newest[:, None, :] - log_gates
    gate_bias = gate_bias.reshape(seqs_here, cache_len, kv_count, group_size).transpose(0, 2, 3, 1)
    past_scores = (
        jnp.einsum("skgd,slkd->skgl", queries, cached_keys, preferred_element_type=jnp.float32)
        * score_scale
        + gate_bias
    )
    is_valid = (current_position[None, :] < lengths[:, None])[:, None, None, :]
    past_scores = jnp.where(is_valid, past_scores, -jnp.inf)
    own_score = (
        jnp.einsum("skgd,skd->skg", queries, key_new, preferred_element_type=jnp.float32)
        * score_scale
    )
    highest = jnp.maximum(jnp.max(past_scores, axis=-1), own_score)
    past_exp = jnp.exp(past_scores - highest[..., None])
    own_exp = jnp.exp(own_score - highest)
    totals = jnp.sum(past_exp, axis=-1) + own_exp
    past_weights = (past_exp / totals[..., None]).astype(jnp.bfloat16)
    own_weights = (own_exp / totals).astype(jnp.bfloat16)
    mixed_values = jnp.einsum(
        "skgl,slkd->skgd", past_weights, cached_values, preferred_element_type=jnp.float32
    )
    mixed_values = (
        mixed_values
        + own_weights.astype(jnp.float32)[..., None] * value_new.astype(jnp.float32)[:, :, None, :]
    )
    return mixed_values.astype(jnp.bfloat16).reshape(seqs_here, kv_count * group_size * head_width)


def swap_bit(value, axis, bit):
    count = lax.axis_size(axis)
    return lax.ppermute(value, axis, [(i, i ^ bit) for i in range(count)])


def bits_of(axis):
    count = lax.axis_size(axis)
    return [1 << k for k in range(count.bit_length() - 1)]


def keep_block(blocks, axis):
    index = lax.axis_index(axis)
    for bit in bits_of(axis):
        count = blocks.shape[0]
        pairs = blocks.reshape((count // 2, 2) + blocks.shape[1:])
        high = (index & bit) > 0
        sent = jnp.where(high, pairs[:, 0], pairs[:, 1]).astype(jnp.bfloat16)
        kept = jnp.where(high, pairs[:, 1], pairs[:, 0]).astype(jnp.float32)
        blocks = kept + swap_bit(sent, axis, bit).astype(jnp.float32)
    return blocks[0]


def narrow(value):
    return lax.reduce_precision(value, 8, 7)


def split_terms(value, count):
    pieces = []
    for _ in range(count):
        piece = narrow(value)
        pieces.append(piece.astype(jnp.bfloat16))
        value = value - piece
    return pieces


def whole(*arrays):
    return [pl.BlockSpec(memory_space=pltpu.VMEM) for _ in arrays]


def norm_kernel(tokens_ref, gain_ref, out_ref):
    values = tokens_ref[...].astype(jnp.float32)
    scale = lax.rsqrt(jnp.mean(values * values, axis=1, keepdims=True) + EPS)
    normed = (values * scale * gain_ref[...]).astype(jnp.bfloat16)
    blocks, _, cols = out_ref.shape
    for block in range(blocks):
        out_ref[block] = normed[:, block * cols : (block + 1) * cols]


def normed_blocks(tokens, gain, blocks):
    rows, width = tokens.shape
    return pl.pallas_call(
        norm_kernel,
        out_shape=jax.ShapeDtypeStruct((blocks, rows, width // blocks), jnp.bfloat16),
        in_specs=whole(tokens, gain),
        out_specs=pl.BlockSpec(memory_space=pltpu.VMEM),
        name="first_norm",
    )(tokens, gain.reshape(1, width))


def attend_kernel(lengths_ref, query_ref, new_ref, forget_ref, cache_ref, gates_ref, out_ref):
    group, heads, lanes = query_ref.shape
    cache_len = cache_ref.shape[1]
    head_width = lanes // 2
    scale = head_width ** (-0.5)
    first = pl.program_id(0) * group
    position = lax.broadcasted_iota(jnp.int32, (heads, cache_len), 1)
    for item in range(group):
        length = lengths_ref[first + item]
        query = query_ref[item]
        cache = cache_ref[item]
        gates = gates_ref[item]
        last_gate = jnp.sum(jnp.where(position == length - 1, gates, 0.0), axis=1, keepdims=True)
        newest = last_gate + forget_ref[item]
        scores = lax.dot_general(
            query, cache, (((1,), (1,)), ((), ())), preferred_element_type=jnp.float32
        )
        scores = scores * scale + (newest - gates)
        scores = jnp.where(position < length, scores, -jnp.inf)
        fresh = new_ref[pl.ds(item, 1), :].astype(jnp.float32)
        own = jnp.sum(query.astype(jnp.float32) * fresh, axis=1, keepdims=True) * scale
        highest = jnp.maximum(jnp.max(scores, axis=1, keepdims=True), own)
        past_exp = jnp.exp(scores - highest)
        own_exp = jnp.exp(own - highest)
        total = jnp.sum(past_exp, axis=1, keepdims=True) + own_exp
        past = (past_exp / total).astype(jnp.bfloat16)
        own_share = (own_exp / total).astype(jnp.bfloat16).astype(jnp.float32)
        mixed = lax.dot_general(
            past, cache, (((1,), (0,)), ((), ())), preferred_element_type=jnp.float32
        )
        out_ref[item] = (mixed + own_share * fresh).astype(jnp.bfloat16)


def attend_fused(queries, key_new, value_new, forget, kv_cache, log_gates, lengths):
    seqs, cache_len, _, lanes = kv_cache.shape
    head_width = lanes // 2
    heads = queries.shape[1] // head_width
    wide = jnp.pad(queries.reshape(seqs, heads, head_width), ((0, 0), (0, 0), (0, head_width)))
    fresh = jnp.concatenate([key_new, value_new], axis=1)
    steps = 4 if seqs % 4 == 0 else 1
    group = seqs // steps
    out = pl.pallas_call(
        attend_kernel,
        out_shape=jax.ShapeDtypeStruct((seqs, heads, lanes), jnp.bfloat16),
        grid_spec=pltpu.PrefetchScalarGridSpec(
            num_scalar_prefetch=1,
            grid=(steps,),
            in_specs=[
                pl.BlockSpec((group, heads, lanes), lambda i, _: (i, 0, 0)),
                pl.BlockSpec((None, group, lanes), lambda i, _: (i, 0, 0)),
                pl.BlockSpec((group, heads, 1), lambda i, _: (i, 0, 0)),
                pl.BlockSpec((group, cache_len, lanes), lambda i, _: (i, 0, 0)),
                pl.BlockSpec((group, heads, cache_len), lambda i, _: (i, 0, 0)),
            ],
            out_specs=pl.BlockSpec((group, heads, lanes), lambda i, _: (i, 0, 0)),
        ),
        cost_estimate=pl.CostEstimate(
            flops=4 * seqs * heads * cache_len * lanes,
            transcendentals=seqs * heads * cache_len,
            bytes_accessed=seqs * cache_len * (2 * lanes + 4 * heads),
        ),
        name="attend",
    )(
        lengths,
        wide,
        fresh.reshape(steps, group, lanes),
        forget[:, :, None],
        kv_cache.reshape(seqs, cache_len, lanes),
        log_gates.transpose(0, 2, 1),
    )
    return out[:, :, head_width:].reshape(seqs, heads * head_width)


def silu(value):
    return value / (1.0 + jnp.exp(-value))


def load_all(pairs, sems):
    copies = [
        pltpu.make_async_copy(source, target, sems.at[i])
        for i, (source, target) in enumerate(pairs)
    ]
    for copy in copies:
        copy.start()
    return copies


def expert_kernel(
    index_ref,
    block0_ref,
    block1_ref,
    block2_ref,
    block3_ref,
    gain_ref,
    vector_ref,
    weight_ref,
    gate_hbm,
    up_hbm,
    down_hbm,
    send_ref,
    keep_ref,
    second_ref,
    value_ref,
    gate_ref,
    up_ref,
    down_ref,
    sems,
):
    index = index_ref[0]
    blocks = (block0_ref, block1_ref, block2_ref, block3_ref)
    sources, rows, cols = block0_ref.shape
    width, units = gate_ref.shape
    chunks = 4
    depth = width // chunks
    quarter = down_ref.shape[2]
    pairs = []
    for k in range(chunks):
        span = pl.ds(k * depth, depth)
        pairs.append((gate_hbm.at[span, :], gate_ref.at[span, :]))
        pairs.append((up_hbm.at[span, :], up_ref.at[span, :]))
    for j in range(4):
        start = pl.multiple_of((index ^ j) * quarter, quarter)
        pairs.append((down_hbm.at[:, pl.ds(start, quarter)], down_ref.at[j]))
    copies = load_all(pairs, sems)

    squares = jnp.zeros((rows, cols), jnp.float32)
    for j in range(4):
        for e in range(sources):
            values = blocks[j][e].astype(jnp.float32)
            squares = squares + values * values
    scale = lax.rsqrt(jnp.sum(squares, axis=1, keepdims=True) / width + EPS)
    logit = jnp.zeros((rows, cols), jnp.float32)
    for j in range(4):
        for e in range(sources):
            start = pl.multiple_of((e * 4 + (index ^ j)) * cols, cols)
            span = pl.ds(start, cols)
            values = blocks[j][e].astype(jnp.float32)
            second = (values * scale * gain_ref[:, span]).astype(jnp.bfloat16)
            second_ref[:, span] = second
            logit = logit + second.astype(jnp.float32) * vector_ref[:, span]
    value = 1.0 / (1.0 + jnp.exp(-jnp.sum(logit, axis=1, keepdims=True)))
    value_ref[...] = jnp.broadcast_to(value, value_ref.shape)

    gate = jnp.zeros((rows, units), jnp.float32)
    up = jnp.zeros((rows, units), jnp.float32)
    for k in range(chunks):
        span = slice(k * depth, (k + 1) * depth)
        left = second_ref[:, span]
        copies[2 * k].wait()
        gate = gate + jnp.dot(left, gate_ref[span, :], preferred_element_type=jnp.float32)
        copies[2 * k + 1].wait()
        up = up + jnp.dot(left, up_ref[span, :], preferred_element_type=jnp.float32)
    hidden = (silu(gate) * up).astype(jnp.bfloat16)
    weight = weight_ref[...]
    for j in (1, 3, 0, 2):
        copies[2 * chunks + j].wait()
        out = jnp.dot(hidden, down_ref[j], preferred_element_type=jnp.float32) * weight
        if j % 2:
            send_ref[j // 2] = out.astype(jnp.bfloat16)
        else:
            keep_ref[j // 2] = out


def expert_fused(index, blocks, gain, vector, weight, gate, up, down):
    sources, rows, cols = blocks[0].shape
    width, units = gate.shape
    quarter = width // 4
    hbm = pl.BlockSpec(memory_space=pltpu.HBM)
    vmem = pl.BlockSpec(memory_space=pltpu.VMEM)
    return pl.pallas_call(
        expert_kernel,
        out_shape=(
            jax.ShapeDtypeStruct((2, rows, quarter), jnp.bfloat16),
            jax.ShapeDtypeStruct((2, rows, quarter), jnp.float32),
            jax.ShapeDtypeStruct((rows, width), jnp.bfloat16),
            jax.ShapeDtypeStruct((rows, 128), jnp.float32),
        ),
        in_specs=[pl.BlockSpec(memory_space=pltpu.SMEM)] + [vmem] * 7 + [hbm] * 3,
        out_specs=[vmem] * 4,
        scratch_shapes=[
            pltpu.VMEM((width, units), jnp.bfloat16),
            pltpu.VMEM((width, units), jnp.bfloat16),
            pltpu.VMEM((4, units, quarter), jnp.bfloat16),
            pltpu.SemaphoreType.DMA((12,)),
        ],
        cost_estimate=pl.CostEstimate(
            flops=6 * rows * width * units, transcendentals=0, bytes_accessed=6 * width * units
        ),
        name="expert",
    )(
        index.reshape(1),
        *blocks,
        gain.reshape(1, width),
        vector.reshape(1, width),
        weight.reshape(rows, 1),
        gate,
        up,
        down,
    )


def dense_kernel(
    second_ref, value_ref, gate_hbm, up_hbm, down_hbm, out_ref, gate_ref, up_ref, down_ref, sems
):
    rows = second_ref.shape[0]
    width, units = gate_ref.shape
    chunks = 4
    depth = width // chunks
    pairs = []
    for k in range(chunks):
        span = pl.ds(k * depth, depth)
        pairs.append((gate_hbm.at[span, :], gate_ref.at[span, :]))
        pairs.append((up_hbm.at[span, :], up_ref.at[span, :]))
    pairs.append((down_hbm, down_ref))
    copies = load_all(pairs, sems)
    gate = jnp.zeros((rows, units), jnp.float32)
    up = jnp.zeros((rows, units), jnp.float32)
    for k in range(chunks):
        span = slice(k * depth, (k + 1) * depth)
        left = second_ref[:, span]
        copies[2 * k].wait()
        gate = gate + jnp.dot(left, gate_ref[span, :], preferred_element_type=jnp.float32)
        copies[2 * k + 1].wait()
        up = up + jnp.dot(left, up_ref[span, :], preferred_element_type=jnp.float32)
    hidden = (silu(gate) * up).astype(jnp.bfloat16)
    copies[2 * chunks].wait()
    out = jnp.dot(hidden, down_ref[...], preferred_element_type=jnp.float32)
    out_ref[...] = out * value_ref[:, :1]


def dense_fused(second, value, gate, up, down):
    rows, width = second.shape
    units = gate.shape[1]
    cols = down.shape[1]
    hbm = pl.BlockSpec(memory_space=pltpu.HBM)
    vmem = pl.BlockSpec(memory_space=pltpu.VMEM)
    return pl.pallas_call(
        dense_kernel,
        out_shape=jax.ShapeDtypeStruct((rows, cols), jnp.float32),
        in_specs=[vmem] * 2 + [hbm] * 3,
        out_specs=vmem,
        scratch_shapes=[
            pltpu.VMEM((width, units), jnp.bfloat16),
            pltpu.VMEM((width, units), jnp.bfloat16),
            pltpu.VMEM((units, cols), jnp.bfloat16),
            pltpu.SemaphoreType.DMA((9,)),
        ],
        cost_estimate=pl.CostEstimate(
            flops=2 * rows * units * (2 * width + cols),
            transcendentals=0,
            bytes_accessed=2 * units * (2 * width + cols),
        ),
        name="dense",
    )(second, value, gate, up, down)


def mix_by_columns(tokens, attended, out_weight):
    experts = lax.axis_size("ep")
    shares = lax.axis_size("tp")
    seq_count, width = tokens.shape
    rows = experts * seq_count
    block_cols = out_weight.shape[1] // shares
    own_tokens = lax.dynamic_index_in_dim(
        tokens.reshape(seq_count, experts, shares, block_cols),
        lax.axis_index("tp"),
        2,
        keepdims=False,
    ).transpose(1, 0, 2)
    sent = jnp.concatenate(
        [jnp.broadcast_to(attended, (experts,) + attended.shape), own_tokens], axis=2
    )
    got = lax.all_to_all(sent, "ep", split_axis=0, concat_axis=0, tiled=True)
    got = got.reshape(rows, -1)
    column_terms = jnp.dot(
        got[:, : attended.shape[1]], out_weight, preferred_element_type=jnp.float32
    )
    attention_out = keep_block(
        column_terms.reshape(rows, shares, block_cols).transpose(1, 0, 2), "tp"
    )
    mixed_block = (got[:, attended.shape[1] :].astype(jnp.float32) + attention_out).astype(
        jnp.bfloat16
    )
    gathered = lax.all_to_all(
        jnp.broadcast_to(mixed_block, (experts, rows, block_cols)),
        "ep",
        split_axis=0,
        concat_axis=0,
        tiled=True,
    )
    blocks = [gathered]
    for bit in bits_of("tp"):
        blocks = blocks + [None] * len(blocks)
    for bit in reversed(bits_of("tp")):
        for j, block in enumerate(list(blocks)):
            if block is not None and blocks[j ^ bit] is None:
                blocks[j ^ bit] = swap_bit(block, "tp", bit)
    return blocks


def own_residual(blocks, seq_count, quarter):
    index = lax.axis_index("tp")
    cols = blocks[0].shape[2]
    sources = quarter // (len(blocks) * cols)
    pieces = jnp.stack(
        [
            lax.dynamic_slice(
                block,
                (index * sources, lax.axis_index("ep") * seq_count, 0),
                (sources, seq_count, cols),
            )
            for block in blocks
        ]
    )
    order = jnp.arange(len(blocks), dtype=jnp.int32) ^ index
    return pieces[order].transpose(2, 1, 0, 3).reshape(seq_count, quarter)


def mix_by_rows(tokens, attended, out_weight):
    column_terms = jnp.dot(
        lax.all_gather(attended, "ep", axis=0, tiled=True),
        out_weight,
        preferred_element_type=jnp.float32,
    )
    summed = lax.all_to_all(
        lax.psum(column_terms, "tp"), "ep", split_axis=0, concat_axis=1, tiled=True
    )
    mixed = (tokens.astype(jnp.float32) + summed).astype(jnp.bfloat16)
    return lax.all_gather(mixed, "ep", axis=0, tiled=True)


def finish(residual, total):
    seq_count, quarter = residual.shape
    returned = lax.all_to_all(
        total.reshape(-1, seq_count, quarter), "ep", split_axis=0, concat_axis=0, tiled=True
    )
    return (
        residual.astype(jnp.float32) + jnp.sum(returned.astype(jnp.float32), axis=0)
    ).astype(jnp.bfloat16)


def shards(
    tokens,
    norm_gain,
    query_weight,
    key_weight,
    value_weight,
    forget_weight,
    forget_bias,
    kv_cache,
    log_gates,
    lengths,
    out_weight,
    mix_gain,
    expert_gate,
    expert_up,
    expert_down,
    routes,
    route_weights,
    dense_gate,
    dense_up,
    dense_down,
    gate_vector,
):
    experts = lax.axis_size("ep")
    shares = lax.axis_size("tp")
    ep_index = lax.axis_index("ep")
    tp_index = lax.axis_index("tp")
    seq_count, width = tokens.shape
    rows = experts * seq_count
    query_cols = query_weight.shape[1]
    key_cols = key_weight.shape[1]
    gate_cols = forget_weight.shape[1]

    normed = normed_blocks(tokens, norm_gain, experts)
    columns = lax.all_to_all(normed, "ep", split_axis=0, concat_axis=0, tiled=True)
    columns = columns.reshape(rows, width // experts)

    own_weight = jnp.sum(
        jnp.where(
            routes[None, :, :] == jnp.arange(experts, dtype=jnp.int32)[:, None, None],
            route_weights[None, :, :],
            0.0,
        ),
        axis=2,
    )
    split = query_cols + 2 * key_cols
    spare = -(split + 2 * gate_cols + 3) % 128
    weights = jnp.concatenate(
        [
            query_weight,
            key_weight,
            value_weight,
            forget_weight,
            forget_weight,
            jnp.zeros((query_weight.shape[0], 3 + spare), jnp.bfloat16),
        ],
        axis=1,
    )
    extra = jnp.pad(
        jnp.stack(split_terms(own_weight, 3), axis=2),
        ((0, 0), (0, 0), (split + 2 * gate_cols, spare)),
    ).reshape(rows, -1)
    terms = jnp.dot(columns, weights, preferred_element_type=jnp.float32)
    lane = lax.broadcasted_iota(jnp.int32, terms.shape, 1)
    second_term = (lane >= split + gate_cols) & (lane < split + 2 * gate_cols)
    sent = jnp.where(second_term, terms - narrow(terms), terms).astype(jnp.bfloat16)
    sent = jnp.where(lane < split + 2 * gate_cols, sent, extra)
    got = lax.all_to_all(
        sent.reshape(experts, seq_count, -1), "ep", split_axis=0, concat_axis=0, tiled=True
    )
    projected = jnp.sum(got[:, :, : split + 2 * gate_cols].astype(jnp.float32), axis=0)
    spot = split + 2 * gate_cols
    expert_weight = jnp.sum(got[:, :, spot : spot + 3].astype(jnp.float32), axis=2)
    queries = projected[:, :query_cols].astype(jnp.bfloat16)
    key_new = projected[:, query_cols : query_cols + key_cols].astype(jnp.bfloat16)
    value_new = projected[:, query_cols + key_cols : split].astype(jnp.bfloat16)
    forget = jax.nn.log_sigmoid(
        projected[:, split : split + gate_cols] + projected[:, split + gate_cols :] + forget_bias
    )
    if kv_cache.shape[2] == 1 and 2 * key_cols == 128:
        attended = attend_fused(
            queries, key_new, value_new, forget, kv_cache, log_gates, lengths
        )
    else:
        attended = attend_local(
            queries, key_new, value_new, forget, kv_cache, log_gates, lengths
        )

    capacity = max(2, 2 * seq_count * routes.shape[1] // experts)
    quarter = width // shares
    if out_weight.shape[1] == 128 * shares and shares == 4 and capacity >= seq_count:
        blocks = mix_by_columns(tokens, attended, out_weight)
        residual = own_residual(blocks, seq_count, quarter)
        send, keep, second, value = expert_fused(
            tp_index,
            blocks,
            mix_gain,
            gate_vector,
            expert_weight,
            expert_gate[0],
            expert_up[0],
            expert_down[0],
        )
        across = swap_bit(send, "tp", 1)
        far = swap_bit((keep[1] + across[1].astype(jnp.float32)).astype(jnp.bfloat16), "tp", 2)
        dense_terms = dense_fused(second, value, dense_gate, dense_up, dense_down)
        expert_sum = keep[0] + across[0].astype(jnp.float32) + far.astype(jnp.float32)
        total = (expert_sum + dense_terms).astype(jnp.bfloat16)
        return finish(residual, total)
    mixed = mix_by_rows(tokens, attended, out_weight)
    second = rms_scaled(mixed, mix_gain).astype(jnp.bfloat16)
    gate_value = jax.nn.sigmoid(jnp.sum(second.astype(jnp.float32) * gate_vector, axis=1))

    weight = expert_weight
    picked = second
    chooser = None
    if capacity < seq_count:
        taken = weight > 0
        place = jnp.cumsum(taken.astype(jnp.int32), axis=1) - 1
        chooser = (
            taken[:, None, :]
            & (place[:, None, :] == jnp.arange(capacity, dtype=jnp.int32)[None, :, None])
        ).astype(jnp.bfloat16)
        picked = jnp.einsum(
            "ecs,esd->ecd",
            chooser,
            second.reshape(experts, seq_count, width),
            preferred_element_type=jnp.float32,
        ).astype(jnp.bfloat16)
        picked = picked.reshape(experts * capacity, width)
        weight = jnp.einsum(
            "ecs,es->ec",
            chooser.astype(jnp.float32),
            weight,
            precision=lax.Precision.HIGHEST,
        )
    gate_pre = jnp.dot(picked, expert_gate[0], preferred_element_type=jnp.float32)
    up_pre = jnp.dot(picked, expert_up[0], preferred_element_type=jnp.float32)
    hidden = (jax.nn.silu(gate_pre) * up_pre).astype(jnp.bfloat16)
    expert_out = jnp.dot(hidden, expert_down[0], preferred_element_type=jnp.float32)
    expert_out = expert_out * weight.reshape(-1)[:, None]
    served = expert_out.shape[0]
    expert_sum = keep_block(
        expert_out.reshape(served, shares, quarter).transpose(1, 0, 2), "tp"
    )
    if chooser is not None:
        expert_sum = jnp.einsum(
            "ecs,ecd->esd",
            chooser,
            expert_sum.reshape(experts, capacity, quarter).astype(jnp.bfloat16),
            preferred_element_type=jnp.float32,
        ).reshape(rows, quarter)

    dense_hidden = (
        jax.nn.silu(jnp.dot(second, dense_gate, preferred_element_type=jnp.float32))
        * jnp.dot(second, dense_up, preferred_element_type=jnp.float32)
    ).astype(jnp.bfloat16)
    dense_terms = jnp.dot(dense_hidden, dense_down, preferred_element_type=jnp.float32)
    total = (expert_sum + gate_value[:, None] * dense_terms).astype(jnp.bfloat16)

    residual = lax.dynamic_slice(
        mixed, (ep_index * seq_count, tp_index * quarter), (seq_count, quarter)
    )
    return finish(residual, total)


def solution(mesh):
    return jax.shard_map(
        shards,
        mesh=mesh,
        in_specs=(
            P("ep", None),
            P(),
            P("ep", "tp"),
            P("ep", "tp"),
            P("ep", "tp"),
            P("ep", "tp"),
            P("tp"),
            P("ep", None, "tp", None),
            P("ep", None, "tp"),
            P("ep"),
            P("tp", "ep"),
            P(),
            P("ep", None, "tp"),
            P("ep", None, "tp"),
            P("ep", "tp", None),
            P("ep", None),
            P("ep", None),
            P(None, "ep"),
            P(None, "ep"),
            P("ep", "tp"),
            P(),
        ),
        out_specs=P("ep", "tp"),
        check_vma=False,
    )
```

time: 334 us -> 115 us (0.34)
  waiting for transfers between devices: 221 us -> 35.3 us
  blocking collectives: 44.9 us -> 10.9 us
  matrix products: 26.6 us -> 1.2 us
  Pallas kernels: 0 us -> 24.5 us
  between operations: 13.5 us -> 0.26 us
  local copies, waits for them, and re-layouts: 1.59 us -> 12.6 us
  starting transfers between devices: 14.8 us -> 24 us
  other arithmetic: 10.4 us -> 5.41 us
    reduce_scatter x3 -> x0, waiting for transfers between devices: 132 us -> none  [the longest x1 59.1 us: shards(): lax.psum_scatter(jnp.concatenate([jnp.dot(row_block, matrix, preferred_el...]
    psum x1 -> x0, waiting for transfers between devices: 31.3 us -> none  [shards(): column_total = lax.psum(column_terms, 'tp')]
    all_gather x1 -> x0, blocking collectives: 30.5 us -> none  [shards(): lax.all_gather(attended, 'ep', axis=0, tiled=True)]
    dot_general x14 -> x2, matrix products: 26.6 us -> 1.2 us  [the longest x1 0.97 us: shards(): terms = jnp.dot(columns, weights, preferred_element_type=jnp.float32)]
    pallas_call x0 -> x4, Pallas kernels: none -> 24.5 us  [the longest x1 9.14 us: attend_fused(): pl.pallas_call(attend_kernel, out_shape=jax.ShapeDtypeStruct((seqs, heads...]
    all_to_all x3 -> x4, waiting for transfers between devices: 43.6 us -> 24.2 us  [the longest x1 7.6 us: shards(): lax.all_to_all(sent.reshape(experts, seq_count, -1), 'ep', split_axis=0,...]
    all_gather x1 -> x0, waiting for transfers between devices: 14 us -> none  [shards(): piece = lax.all_gather(second, 'ep', axis=0, tiled=True)]
    ppermute x0 -> x7, waiting for transfers between devices: none -> 11.1 us  [swap_bit(): return lax.ppermute(value, axis, [(i, i ^ bit) for i in range(count)])]
  transfers between devices with their start and end apart: 8 -> 11, of which waited for: 8 -> 9; matrix products, arithmetic and copies ran while one was open for 6% -> 8% of each run, Pallas kernels for 0% -> 5%
where the time goes in v1:
time: 115 us; the launch traced here: 114 us
  waiting for transfers between devices  35.3 us (31%)
  Pallas kernels  24.5 us (21%)
  starting transfers between devices  24 us (21%)
  local copies, waits for them, and re-layouts  12.6 us (11%)
  blocking collectives  10.9 us (9%)
  other arithmetic  5.41 us (5%)
  matrix products  1.2 us (1%)
    ppermute x7, waiting for transfers between devices, swap_bit(): return lax.ppermute(value, axis, [(i, i ^ bit) for i in range(count)])  11.1 us
    all_to_all x1, blocking collectives, mix_by_columns(): lax.all_to_all(jnp.broadcast_to(mixed_block, (experts, rows, block_cols))...  10.9 us
    pallas_call x1, Pallas kernels, attend_fused(): pl.pallas_call(attend_kernel, out_shape=jax.ShapeDtypeStruct((seqs, heads...  9.14 us
    all_to_all x1, waiting for transfers between devices, shards(): lax.all_to_all(sent.reshape(experts, seq_count, -1), 'ep', split_axis=0,...  7.6 us
    all_to_all x1, waiting for transfers between devices, mix_by_columns(): got = lax.all_to_all(sent, 'ep', split_axis=0, concat_axis=0, tiled=True)  7.49 us
    pallas_call x1, Pallas kernels, expert_fused(): pl.pallas_call(expert_kernel, out_shape=(jax.ShapeDtypeStruct((2, rows, q...  7.32 us
    all_to_all x1, starting transfers between devices, shards(): lax.all_to_all(normed, 'ep', split_axis=0, concat_axis=0, tiled=True)  7.28 us
    all_to_all x1, waiting for transfers between devices, finish(): lax.all_to_all(total.reshape(-1, seq_count, quarter), 'ep', split_axis=0,...  6.86 us
  transfers between devices with their start and end apart: 11, of which 9 were waited for; matrix products, arithmetic and copies ran while one was open for 8% of the time, Pallas kernels for 5%

profile of v1, /device:TPU:0, one launch (start us, length us, event | category | flops | bytes accessed | tf_op | source)
XLA Modules:
  0.0 114.3 jit_solution(6129694137284855896)
XLA Ops:
  0.0 1.8 %first_norm.1 = bf16[8,16,512]{2,1,0:T(8,128)(2,1)} custom-call(bf16[16,4096]{1,0:T(8,128)(2,1)} %tokens_ref.1, f32[1,4096]{1,0:T(1,128)} %bitcast.111), custom_call_target="tpu_custom_call" | custom-call | tf_op jit(solution)/shard_map/first_norm/pallas_call | solution.py:109
  1.8 7.3 %all-to-all-start = ((bf16[8,16,512]{2,1,0:T(8,128)(2,1)}), bf16[8,16,512]{2,1,0:T(8,128)(2,1)S(1)}, u32[]{:S(2)}, u32[]{:S(2)}) async-start(bf16[8,16,512]{2,1,0:T(8,128)(2,1)} %first_norm.1), calls=%async_computation | async-start | bytes 262144 | tf_op jit(solution)/shard_map/all_to_all | solution.py:492
  9.1 0.7 select_reduce_fusion
  9.8 0.1 copy.120
  9.9 1.0 copy.100
  10.9 1.0 copy.101
  11.9 0.9 copy.102
  12.8 1.3 %concatenate.9 = bf16[512,768]{1,0:T(8,128)(2,1)S(1)} concatenate(bf16[512,512]{1,0:T(8,128)(2,1)} %param.23, bf16[512,64]{1,0:T(8,128)(2,1)S(1)} %copy.100, bf16[512,64]{1,0:T(8,128)(2,1)S(1)} %copy.101, bf16[512,8]{1,0:T(8,128)(2,1)S(1)} %copy.102, bf16[512,8]{1,0:T(8,128)(2,1)S(1)} %copy.102, bf16[512,112]{1,0:T(8,128)(2,1)S(1)} %broadcast_in_dim.29), dimensions={1} | concatenate | bytes 1572864 | tf_op jit(solution)/shard_map/concatenate | solution.py:505
  14.1 2.3 %all-to-all-done = bf16[8,16,512]{2,1,0:T(8,128)(2,1)S(1)} async-done(((bf16[8,16,512]{2,1,0:T(8,128)(2,1)}), bf16[8,16,512]{2,1,0:T(8,128)(2,1)S(1)}, u32[]{:S(2)}, u32[]{:S(2)}) %all-to-all-start) | async-done | bytes 131104 | tf_op jit(solution)/shard_map/all_to_all | solution.py:492
  16.4 1.0 fusion.4
  17.4 3.7 %all-to-all-start.1 = ((bf16[8,16,768]{2,1,0:T(8,128)(2,1)}), bf16[8,16,768]{2,1,0:T(8,128)(2,1)S(1)}, u32[]{:S(2)}, u32[]{:S(2)}) async-start(bf16[8,16,768]{2,1,0:T(8,128)(2,1)} %bitcast.4), calls=%async_computation.1 | async-start | bytes 393216 | tf_op jit(solution)/shard_map/all_to_all | solution.py:525
  21.3 7.6 %all-to-all-done.1 = bf16[8,16,768]{2,1,0:T(8,128)(2,1)S(1)} async-done(((bf16[8,16,768]{2,1,0:T(8,128)(2,1)}), bf16[8,16,768]{2,1,0:T(8,128)(2,1)S(1)}, u32[]{:S(2)}, u32[]{:S(2)}) %all-to-all-start.1) | async-done | bytes 196640 | tf_op jit(solution)/shard_map/all_to_all | solution.py:525
  29.0 0.6 slice.84
  29.8 0.1 reshape.175
  29.8 0.6 pad.9.query_ref
  30.6 0.8 copy.107.forget_ref
  31.3 9.1 %attend.1 = bf16[16,8,128]{2,1,0:T(8,128)(2,1)} custom-call(s32[16]{0:T(128)} %lengths_ref.1, bf16[16,8,128]{2,1,0:T(8,128)(2,1)} %pad.9.query_ref, bf16[4,4,128]{2,1,0:T(4,128)(2,1)} %bitcast.112, f32[16,8,1]{2,1,0:T(8,128)} %copy.107.forget_ref, bf16[16,1024,128]{2,1,0:T(8,128)(2,1)} %bitcast.98, f32[16,8,1024]{2,1,0:T(8,128)} %bitcast.106), custom_call_target="tpu_custom_call" | custom-call | flops 67108864 | bytes 4718592 | tf_op jit(solution)/shard_map/attend/pallas_call | solution.py:159
  40.5 0.8 slice.87
  41.3 0.1 reshape.178
  41.4 0.7 pad_maximum_fusion
  42.1 3.4 %all-to-all-start.2 = ((bf16[8,16,640]{2,1,0:T(8,128)(2,1)}), bf16[8,16,640]{2,1,0:T(8,128)(2,1)S(1)}, u32[]{:S(2)}, u32[]{:S(2)}) async-start(bf16[8,16,640]{2,1,0:T(8,128)(2,1)} %pad_maximum_fusion), calls=%async_computation.2 | async-start | bytes 327680 | tf_op jit(solution)/shard_map/all_to_all | solution.py:389
  45.5 7.5 %all-to-all-done.2 = bf16[8,16,640]{2,1,0:T(8,128)(2,1)S(1)} async-done(((bf16[8,16,640]{2,1,0:T(8,128)(2,1)}), bf16[8,16,640]{2,1,0:T(8,128)(2,1)S(1)}, u32[]{:S(2)}, u32[]{:S(2)}) %all-to-all-start.2) | async-done | bytes 163872 | tf_op jit(solution)/shard_map/all_to_all | solution.py:389
  53.0 0.2 convolution_bitcast_fusion
  53.3 1.2 %collective-permute-done = bf16[2,128,128]{2,1,0:T(8,128)(2,1)S(1)} collective-permute-done((bf16[2,128,128]{2,1,0:T(8,128)(2,1)S(1)}, bf16[2,128,128]{2,1,0:T(8,128)(2,1)S(1)}, u32[]{:S(2)}, u32[]{:S(2)}) %collective-permute-start) | collective-permute-done | bytes 65568 | tf_op jit(solution)/shard_map/ppermute | solution.py:61
  54.6 1.6 %collective-permute-start.1 = (bf16[1,128,128]{2,1,0:T(8,128)(2,1)S(1)}, bf16[1,128,128]{2,1,0:T(8,128)(2,1)S(1)}, u32[]{:S(2)}, u32[]{:S(2)}) collective-permute-start(bf16[1,128,128]{2,1,0:T(8,128)(2,1)S(1)} %fusion.11), channel_id=1, source_target_pairs={{0,2},{1,3},{2,0},{3,1},{4,6},{5,7},{6,4},{7,5},{8,10},{9,11},{10,... | collective-permute-start | bytes 98312 | tf_op jit(solution)/shard_map/ppermute | solution.py:61
  56.2 2.4 %collective-permute-done.1 = bf16[1,128,128]{2,1,0:T(8,128)(2,1)S(1)} collective-permute-done((bf16[1,128,128]{2,1,0:T(8,128)(2,1)S(1)}, bf16[1,128,128]{2,1,0:T(8,128)(2,1)S(1)}, u32[]{:S(2)}, u32[]{:S(2)}) %collective-permute-start.1) | collective-permute-done | bytes 32800 | tf_op jit(solution)/shard_map/ppermute | solution.py:61
  58.7 10.9 %all_to_all.25.block0_ref = bf16[8,128,128]{2,1,0:T(8,128)(2,1)S(1)} all-to-all(bf16[8,128,128]{2,1,0:T(8,128)(2,1)S(1)} %broadcast_in_dim.34), channel_id=1, replica_groups=mesh['ep'=8,'tp'=4] {'ep'}, dimensions={0} | all-to-all | bytes 524288 | tf_op jit(solution)/shard_map/all_to_all | solution.py:400
  69.6 1.5 %collective-permute-start.3 = (bf16[8,128,128]{2,1,0:T(8,128)(2,1)S(1)}, bf16[8,128,128]{2,1,0:T(8,128)(2,1)S(1)}, u32[]{:S(2)}, u32[]{:S(2)}) collective-permute-start(bf16[8,128,128]{2,1,0:T(8,128)(2,1)S(1)} %all_to_all.25.block0_ref), channel_id=1, source_target_pairs={{0,2},{1,3},{2,0},{3,1},{4,6},{5,7},{6,4},{7,5},{8,10},{9,11},{10,... | collective-permute-start | bytes 786440 | tf_op jit(solution)/shard_map/ppermute | solution.py:61
  71.1 4.8 %collective-permute-done.3.block2_ref = bf16[8,128,128]{2,1,0:T(8,128)(2,1)S(1)} collective-permute-done((bf16[8,128,128]{2,1,0:T(8,128)(2,1)S(1)}, bf16[8,128,128]{2,1,0:T(8,128)(2,1)S(1)}, u32[]{:S(2)}, u32[]{:S(2)}) %collective-permute-start.3) | collective-permute-done | bytes 262176 | tf_op jit(solution)/shard_map/ppermute | solution.py:61
  76.0 0.2 convert_reduce_fusion.2
  76.1 0.7 reshape.198.weight_ref
  76.9 0.7 collective-permute-done.4.block3_ref
  77.6 0.7 copy-done.5
  78.2 7.3 %expert.1 = (bf16[2,128,1024]{2,1,0:T(8,128)(2,1)}, f32[2,128,1024]{2,1,0:T(8,128)}, bf16[128,4096]{1,0:T(8,128)(2,1)}, f32[128,128]{1,0:T(8,128)}) custom-call(s32[1]{0:T(128)} %bitcast.29.index_ref, bf16[8,128,128]{2,1,0:T(8,128)(2,1)} %copy-done.1, bf16[8,128,128]{2,1,0:T(8,128)(2,1)} %copy-done.4, bf16[8,128,128]{2,1,0:T(8,128)(2,1)} %copy-done.6, ...), custom_call_target="tpu_custom_call" | custom-call | flops 805306368 | bytes 6291456 | tf_op jit(solution)/shard_map/expert/pallas_call | solution.py:287
  85.6 0.2 collective-permute-start.5
  85.8 2.0 %collective-permute-done.5 = bf16[2,128,1024]{2,1,0:T(8,128)(2,1)S(1)} collective-permute-done((bf16[2,128,1024]{2,1,0:T(8,128)(2,1)}, bf16[2,128,1024]{2,1,0:T(8,128)(2,1)S(1)}, u32[]{:S(2)}, u32[]{:S(2)}) %collective-permute-start.5) | collective-permute-done | bytes 524320 | tf_op jit(solution)/shard_map/ppermute | solution.py:61
  87.7 1.1 fusion.3
  88.8 1.6 %collective-permute-start.6 = (bf16[128,1024]{1,0:T(8,128)(2,1)S(1)}, bf16[128,1024]{1,0:T(8,128)(2,1)S(1)}, u32[]{:S(2)}, u32[]{:S(2)}) collective-permute-start(bf16[128,1024]{1,0:T(8,128)(2,1)S(1)} %fusion.3), channel_id=1, source_target_pairs={{0,2},{1,3},{2,0},{3,1},{4,6},{5,7},{6,4},{7,5},{8,10},{9,11},{10,... | collective-permute-start | bytes 786440 | tf_op jit(solution)/shard_map/ppermute | solution.py:61
  90.4 0.7 dynamic-slice_bitcast_fusion.3
  91.1 0.7 dynamic-slice_bitcast_fusion.1
  91.8 6.2 %dense.1 = f32[128,1024]{1,0:T(8,128)} custom-call(bf16[128,4096]{1,0:T(8,128)(2,1)} %get-tuple-element.11.second_ref, f32[128,128]{1,0:T(8,128)} %get-tuple-element.12.value_ref, bf16[4096,512]{1,0:T(8,128)(2,1)} %gate_hbm.1, bf16[4096,512]{1,0:T(8,128)(2,1)} %up_hbm.1, bf16[512,1024]{1,0:T(8,128)(2,1)} %down_hbm.1), custom_call_target="tpu_custom_call" | custom-call | flops 1207959552 | bytes 9437184 | tf_op jit(solution)/shard_map/dense/pallas_call | solution.py:354
  98.1 1.9 %fusion.1 = bf16[128,1024]{1,0:T(8,128)(2,1)} fusion(f32[128,1024]{1,0:T(8,128)} %dense.1, bf16[128,1024]{1,0:T(8,128)(2,1)S(1)} %collective-permute-done.6, f32[2,128,1024]{2,1,0:T(8,128)S(1)} %copy-done.2, bf16[2,128,1024]{2,1,0:T(8,128)(2,1)S(1)} %collective-permute-done.5), kind=kLoop, calls=%fused_computation.5 | loop fusion | flops 786432 | bytes 1835008 | tf_op jit(solution)/shard_map/convert_element_type | solution.py:565
  100.0 4.7 %all-to-all-start.4 = ((bf16[8,16,1024]{2,1,0:T(8,128)(2,1)}), bf16[8,16,1024]{2,1,0:T(8,128)(2,1)S(1)}, u32[]{:S(2)}, u32[]{:S(2)}) async-start(bf16[8,16,1024]{2,1,0:T(8,128)(2,1)} %bitcast.37), calls=%async_computation.4 | async-start | bytes 524288 | tf_op jit(solution)/shard_map/all_to_all | solution.py:450
  104.6 0.7 dynamic-slice_bitcast_fusion.2
  105.4 0.7 dynamic-slice_bitcast_fusion
  106.1 0.6 gather_fusion
  106.7 6.9 %all-to-all-done.4 = bf16[8,16,1024]{2,1,0:T(8,128)(2,1)S(1)} async-done(((bf16[8,16,1024]{2,1,0:T(8,128)(2,1)}), bf16[8,16,1024]{2,1,0:T(8,128)(2,1)S(1)}, u32[]{:S(2)}, u32[]{:S(2)}) %all-to-all-start.4) | async-done | bytes 262176 | tf_op jit(solution)/shard_map/all_to_all | solution.py:450
  113.6 0.6 add_convert_fusion.1
  (49 shorter events, 1.1 us)
Async XLA Ops:
  0.0 53.0 %copy-start = (bf16[512,512]{1,0:T(8,128)(2,1)S(1)}, bf16[512,512]{1,0:T(8,128)(2,1)}, u32[]{:S(2)}) copy-start(bf16[512,512]{1,0:T(8,128)(2,1)} %param.31) | copy-start | bytes 1572868
  0.0 21.1 %copy-start.3 = (bf16[16,4096]{1,0:T(8,128)(2,1)S(1)}, bf16[16,4096]{1,0:T(8,128)(2,1)}, u32[]{:S(2)}) copy-start(bf16[16,4096]{1,0:T(8,128)(2,1)} %tokens_ref.1) | copy-start | bytes 393220
  0.0 30.5 %copy-start.7 = (f32[8]{0:T(128)S(1)}, f32[8]{0:T(128)}, u32[]{:S(2)}) copy-start(f32[8]{0:T(128)} %param.27) | copy-start | bytes 100
  1.8 14.6 %all-to-all-start = ((bf16[8,16,512]{2,1,0:T(8,128)(2,1)}), bf16[8,16,512]{2,1,0:T(8,128)(2,1)S(1)}, u32[]{:S(2)}, u32[]{:S(2)}) async-start(bf16[8,16,512]{2,1,0:T(8,128)(2,1)} %first_norm.1), calls=%async_computation | async-start | bytes 262144 | tf_op jit(solution)/shard_map/all_to_all | solution.py:492
  17.4 11.5 %all-to-all-start.1 = ((bf16[8,16,768]{2,1,0:T(8,128)(2,1)}), bf16[8,16,768]{2,1,0:T(8,128)(2,1)S(1)}, u32[]{:S(2)}, u32[]{:S(2)}) async-start(bf16[8,16,768]{2,1,0:T(8,128)(2,1)} %bitcast.4), calls=%async_computation.1 | async-start | bytes 393216 | tf_op jit(solution)/shard_map/all_to_all | solution.py:525
  42.1 10.9 %all-to-all-start.2 = ((bf16[8,16,640]{2,1,0:T(8,128)(2,1)}), bf16[8,16,640]{2,1,0:T(8,128)(2,1)S(1)}, u32[]{:S(2)}, u32[]{:S(2)}) async-start(bf16[8,16,640]{2,1,0:T(8,128)(2,1)} %pad_maximum_fusion), calls=%async_computation.2 | async-start | bytes 327680 | tf_op jit(solution)/shard_map/all_to_all | solution.py:389
  53.3 1.3 %collective-permute-start = (bf16[2,128,128]{2,1,0:T(8,128)(2,1)S(1)}, bf16[2,128,128]{2,1,0:T(8,128)(2,1)S(1)}, u32[]{:S(2)}, u32[]{:S(2)}) collective-permute-start(bf16[2,128,128]{2,1,0:T(8,128)(2,1)S(1)} %fusion.9), channel_id=1, source_target_pairs={{0,1},{1,0},{2,3},{3,2},{4,5},{5,4},{6,7},{7,6},{8,9},{9,8},{10,11... | collective-permute-start | bytes 196616 | tf_op jit(solution)/shard_map/ppermute | solution.py:61
  54.6 4.0 %collective-permute-start.1 = (bf16[1,128,128]{2,1,0:T(8,128)(2,1)S(1)}, bf16[1,128,128]{2,1,0:T(8,128)(2,1)S(1)}, u32[]{:S(2)}, u32[]{:S(2)}) collective-permute-start(bf16[1,128,128]{2,1,0:T(8,128)(2,1)S(1)} %fusion.11), channel_id=1, source_target_pairs={{0,2},{1,3},{2,0},{3,1},{4,6},{5,7},{6,4},{7,5},{8,10},{9,11},{10,... | collective-permute-start | bytes 98312 | tf_op jit(solution)/shard_map/ppermute | solution.py:61
  69.6 7.9 %copy-start.1 = (bf16[8,128,128]{2,1,0:T(8,128)(2,1)}, bf16[8,128,128]{2,1,0:T(8,128)(2,1)S(1)}, u32[]{:S(2)}) copy-start(bf16[8,128,128]{2,1,0:T(8,128)(2,1)S(1)} %all_to_all.25.block0_ref) | copy-start | bytes 786436
  69.6 6.4 %collective-permute-start.3 = (bf16[8,128,128]{2,1,0:T(8,128)(2,1)S(1)}, bf16[8,128,128]{2,1,0:T(8,128)(2,1)S(1)}, u32[]{:S(2)}, u32[]{:S(2)}) collective-permute-start(bf16[8,128,128]{2,1,0:T(8,128)(2,1)S(1)} %all_to_all.25.block0_ref), channel_id=1, source_target_pairs={{0,2},{1,3},{2,0},{3,1},{4,6},{5,7},{6,4},{7,5},{8,10},{9,11},{10,... | collective-permute-start | bytes 786440 | tf_op jit(solution)/shard_map/ppermute | solution.py:61
  71.1 5.7 %collective-permute-start.2 = (bf16[8,128,128]{2,1,0:T(8,128)(2,1)S(1)}, bf16[8,128,128]{2,1,0:T(8,128)(2,1)S(1)}, u32[]{:S(2)}, u32[]{:S(2)}) collective-permute-start(bf16[8,128,128]{2,1,0:T(8,128)(2,1)S(1)} %all_to_all.25.block0_ref), channel_id=1, source_target_pairs={{0,1},{1,0},{2,3},{3,2},{4,5},{5,4},{6,7},{7,6},{8,9},{9,8},{10,11... | collective-permute-start | bytes 786440 | tf_op jit(solution)/shard_map/ppermute | solution.py:61
  76.0 1.5 %copy-start.6 = (bf16[8,128,128]{2,1,0:T(8,128)(2,1)}, bf16[8,128,128]{2,1,0:T(8,128)(2,1)S(1)}, u32[]{:S(2)}) copy-start(bf16[8,128,128]{2,1,0:T(8,128)(2,1)S(1)} %collective-permute-done.3.block2_ref) | copy-start | bytes 786436
  76.0 1.5 %collective-permute-start.4 = (bf16[8,128,128]{2,1,0:T(8,128)(2,1)S(1)}, bf16[8,128,128]{2,1,0:T(8,128)(2,1)S(1)}, u32[]{:S(2)}, u32[]{:S(2)}) collective-permute-start(bf16[8,128,128]{2,1,0:T(8,128)(2,1)S(1)} %collective-permute-done.3.block2_ref), channel_id=1, source_target_pairs={{0,1},{1,0},{2,3},{3,2},{4,5},{5,4},{6,7},{7,6},{8,9},{9,8},{10,11... | collective-permute-start | bytes 786440 | tf_op jit(solution)/shard_map/ppermute | solution.py:61
  76.9 0.7 copy-start.4
  77.5 0.7 copy-start.5
  85.6 2.2 %collective-permute-start.5 = (bf16[2,128,1024]{2,1,0:T(8,128)(2,1)}, bf16[2,128,1024]{2,1,0:T(8,128)(2,1)S(1)}, u32[]{:S(2)}, u32[]{:S(2)}) collective-permute-start(bf16[2,128,1024]{2,1,0:T(8,128)(2,1)} %get-tuple-element.10), channel_id=1, source_target_pairs={{0,1},{1,0},{2,3},{3,2},{4,5},{5,4},{6,7},{7,6},{8,9},{9,8},{10,11... | collective-permute-start | bytes 1572872 | tf_op jit(solution)/shard_map/ppermute | solution.py:61
  88.8 9.2 %collective-permute-start.6 = (bf16[128,1024]{1,0:T(8,128)(2,1)S(1)}, bf16[128,1024]{1,0:T(8,128)(2,1)S(1)}, u32[]{:S(2)}, u32[]{:S(2)}) collective-permute-start(bf16[128,1024]{1,0:T(8,128)(2,1)S(1)} %fusion.3), channel_id=1, source_target_pairs={{0,2},{1,3},{2,0},{3,1},{4,6},{5,7},{6,4},{7,5},{8,10},{9,11},{10,... | collective-permute-start | bytes 786440 | tf_op jit(solution)/shard_map/ppermute | solution.py:61
  91.8 6.3 %copy-start.2 = (f32[2,128,1024]{2,1,0:T(8,128)S(1)}, f32[2,128,1024]{2,1,0:T(8,128)}, u32[]{:S(2)}) copy-start(f32[2,128,1024]{2,1,0:T(8,128)} %get-tuple-element.9) | copy-start | bytes 3145732
  100.0 13.6 %all-to-all-start.4 = ((bf16[8,16,1024]{2,1,0:T(8,128)(2,1)}), bf16[8,16,1024]{2,1,0:T(8,128)(2,1)S(1)}, u32[]{:S(2)}, u32[]{:S(2)}) async-start(bf16[8,16,1024]{2,1,0:T(8,128)(2,1)} %bitcast.37), calls=%async_computation.4 | async-start | bytes 524288 | tf_op jit(solution)/shard_map/all_to_all | solution.py:450
